TPU v7x, 32 devices: a whole 2x2x4 slice. The times are simulated.
32 devices in a mesh: ep: 8 (over z, y), tp: 4 (over x, core).
Axes of the slice: x: 2, y: 2, z: 4, core: 2. Of those that a mesh axis runs over, the one named last changes fastest.
Arguments:
- queries: bfloat16 [4096, 1024], P('ep', 'tp'), may hold values from -8 to 8
- key_rows: bfloat16 [4096, 1024], P('ep', 'tp'), may hold values from -8 to 8
- value_rows: bfloat16 [4096, 1024], P('ep', 'tp'), may hold values from -6 to 6
- lambdas: float32 [8], P('tp'), may hold values from 0.3 to 0.8
- head_gain: float32 [128], replicated, may hold values from 0.1 to 1.9
- out_weight: bfloat16 [1024, 2048], P('tp'), may hold values from -0.1875 to 0.1875
- moe_input: bfloat16 [4096, 2048], P(('ep', 'tp')), may hold values from -400 to 400
- moe_gain: float32 [2048], replicated, may hold values from 0.1 to 1.9
- routes: int32 [4096, 2], P(('ep', 'tp')), may hold values from 0 to 7, all different within a row; in each aligned block of 128 rows (0 to 127, 128 to 255, ...) at most 40 rows name the same one
- route_logits: float32 [4096, 2], P(('ep', 'tp')), may hold values from -6 to 6
- expert_gate: bfloat16 [8, 2048, 3584], P('ep', None, 'tp'), may hold values from -0.125 to 0.125
- expert_up: bfloat16 [8, 2048, 3584], P('ep', None, 'tp'), may hold values from -0.125 to 0.125
- expert_down: bfloat16 [8, 3584, 2048], P('ep', 'tp'), may hold values from -0.09375 to 0.09375
Outputs:
- mixer_out: bfloat16 [4096, 2048], P(('ep', 'tp'))
- expert_out: bfloat16 [4096, 2048], P(('ep', 'tp'))
Inputs may be any that keep to these rules, and one draw needn't show every extreme that they name: `routes`: each token names 2 different experts. Among the tokens of one device no expert is named more than 40 times, and in every draw some expert is named exactly 40 times by the tokens of some device.
All inputs are finite; a program needn't handle non-finite values.
Results may differ from a plain program's by a relative error of at most 0.014.
Values may be sent and summed in bfloat16 or wider, within the bound.
A program may use at most 128 MiB of HBM per device.

v0:
```python
import jax
import jax.numpy as jnp
from jax import lax
from jax.sharding import PartitionSpec as P

epsilon = 1e-06
init_lambda = 0.2


def capacity(tokens, top_count, experts):
    return max(2, (top_count * tokens * 5 + 4 * experts - 1) // (4 * experts))


def per_device(
    queries,
    key_rows,
    value_rows,
    lambdas,
    head_gain,
    out_weight,
    moe_input,
    moe_gain,
    routes,
    route_logits,
    expert_gate,
    expert_up,
    expert_down,
):
    local_rows = queries.shape[0]
    local_heads = lambdas.shape[0]
    head_size = queries.shape[1] // (2 * local_heads)
    value_size = value_rows.shape[1] // local_heads
    model_width = out_weight.shape[1]
    score_scale = head_size ** (-0.5)
    query_maps = queries.reshape(local_rows, local_heads, 2, head_size)

    def attend_block(running, key_block, value_block):
        maxima, totals, accumulated = running
        key_count = key_block.shape[0]
        key_maps = key_block.reshape(key_count, local_heads, 2, head_size)
        value_heads = value_block.reshape(key_count, local_heads, value_size)
        scores = (
            jnp.einsum("qhid,khid->ihqk", query_maps, key_maps, preferred_element_type=jnp.float32)
            * score_scale
        )
        new_max = jnp.maximum(maxima, jnp.max(scores, axis=-1))
        weights = jnp.exp(scores - new_max[..., None])
        factor = jnp.exp(maxima - new_max)
        totals = totals * factor + jnp.sum(weights, axis=-1)
        accumulated = accumulated * factor[..., None] + jnp.einsum(
            "ihqk,khe->ihqe",
            weights.astype(jnp.bfloat16),
            value_heads,
            preferred_element_type=jnp.float32,
        )
        return (new_max, totals, accumulated)

    initial = (
        jnp.full((2, local_heads, local_rows), -1e30, jnp.float32),
        jnp.zeros((2, local_heads, local_rows), jnp.float32),
        jnp.zeros((2, local_heads, local_rows, value_size), jnp.float32),
    )
    key_piece = lax.all_gather(key_rows, "ep", axis=0, tiled=True)
    value_piece = lax.all_gather(value_rows, "ep", axis=0, tiled=True)
    length = key_piece.shape[0]
    block_rows = length
    while block_rows > 1024 and block_rows % 2 == 0:
        block_rows //= 2

    def loop_body(step_index, partial_state):
        first_row = step_index * block_rows
        return attend_block(
            partial_state,
            lax.dynamic_slice_in_dim(key_piece, first_row, block_rows, 0),
            lax.dynamic_slice_in_dim(value_piece, first_row, block_rows, 0),
        )

    maxima, totals, accumulated = lax.fori_loop(0, length // block_rows, loop_body, initial)
    maps_out = accumulated / totals[..., None]
    head_out = maps_out[0] - lambdas[:, None, None] * maps_out[1]
    mean_square = jnp.mean(head_out * head_out, axis=-1, keepdims=True)
    attended = (
        head_out * lax.rsqrt(mean_square + epsilon) * head_gain * (1.0 - init_lambda)
    ).astype(jnp.bfloat16)
    out_heads = out_weight.reshape(local_heads, value_size, model_width)
    token_count, top_count = routes.shape
    experts_all = lax.axis_size("ep")
    slot_count = capacity(token_count, top_count, experts_all)
    moe_float = moe_input.astype(jnp.float32)
    normed = (
        moe_float
        * lax.rsqrt(jnp.mean(moe_float * moe_float, axis=-1, keepdims=True) + epsilon)
        * moe_gain
    ).astype(jnp.bfloat16)
    gate_weights = jax.nn.softmax(route_logits, axis=-1)
    flat_routes = routes.reshape(-1)
    chosen = (flat_routes[:, None] == jnp.arange(experts_all, dtype=jnp.int32)[None, :]).astype(
        jnp.int32
    )
    slot_rank = jnp.sum((jnp.cumsum(chosen, axis=0) - chosen) * chosen, axis=1)
    slot_ids = (flat_routes * slot_count + slot_rank).reshape(token_count, top_count)
    dispatch = jnp.any(
        slot_ids[None, :, :]
        == jnp.arange(experts_all * slot_count, dtype=jnp.int32)[:, None, None],
        axis=-1,
    ).astype(jnp.bfloat16)
    outgoing = (
        jnp.dot(dispatch, normed, preferred_element_type=jnp.float32)
        .astype(jnp.bfloat16)
        .reshape(experts_all, slot_count, model_width)
    )
    gate_local = expert_gate[0]
    up_local = expert_up[0]
    down_local = expert_down[0]
    arrived = lax.all_to_all(outgoing, "ep", split_axis=0, concat_axis=0, tiled=True)
    segment = lax.all_gather(
        arrived.reshape(experts_all * slot_count, model_width), "tp", axis=0, tiled=True
    )
    gate_part = jnp.dot(segment, gate_local, preferred_element_type=jnp.float32)
    up_part = jnp.dot(segment, up_local, preferred_element_type=jnp.float32)
    hidden = (jax.nn.silu(gate_part) * up_part).astype(jnp.bfloat16)
    expert_slots = experts_all * slot_count
    mixer_sum = lax.psum_scatter(
        jnp.einsum("hqe,hed->qd", attended, out_heads, preferred_element_type=jnp.float32).astype(
            jnp.bfloat16
        ),
        "tp",
        scatter_dimension=0,
        tiled=True,
    )
    expert_sum = lax.psum_scatter(
        jnp.dot(hidden, down_local, preferred_element_type=jnp.float32).astype(jnp.bfloat16),
        "tp",
        scatter_dimension=0,
        tiled=True,
    )
    replies = lax.all_to_all(
        expert_sum.reshape(experts_all, slot_count, model_width),
        "ep",
        split_axis=0,
        concat_axis=0,
        tiled=True,
    )
    picked = jnp.take(
        replies.reshape(expert_slots, model_width), slot_ids.reshape(-1), axis=0
    ).reshape(token_count, top_count, model_width)
    expert_out = jnp.sum(gate_weights[:, :, None] * picked.astype(jnp.float32), axis=1).astype(
        jnp.bfloat16
    )
    return (mixer_sum, expert_out)


def solution(mesh):
    placed = (
        P("ep", "tp"),
        P("ep", "tp"),
        P("ep", "tp"),
        P("tp"),
        P(),
        P("tp", None),
        P(("ep", "tp"), None),
        P(),
        P(("ep", "tp"), None),
        P(("ep", "tp"), None),
        P("ep", None, "tp"),
        P("ep", None, "tp"),
        P("ep", "tp", None),
    )
    return jax.shard_map(
        per_device,
        mesh=mesh,
        in_specs=placed,
        out_specs=(P(("ep", "tp"), None), P(("ep", "tp"), None)),
        check_vma=False,
    )
```

profile of v0, /device:TPU:0, one launch (start us, length us, event | category | flops | bytes accessed | tf_op | source)
XLA Modules:
  0.0 297.8 jit_solution(2833831292782214418)
XLA Ops:
  7.2 0.0 copy-start
  7.2 0.0 all-gather.8.cloned.1.call-start
  7.2 0.9 copy.64
  8.1 0.1 eq.39
  8.3 0.1 reshape.131
  8.4 0.6 reduce-window.6
  9.0 0.2 slice_reduce_fusion
  9.3 0.1 fusion.33
  9.4 0.1 reduce_sum.65
  9.5 0.1 copy.66
  9.6 0.7 compare_and_fusion
  10.3 1.2 fusion.19
  11.6 1.6 convolution_convert_fusion.1
  13.2 38.6 %all_to_all.10 = bf16[8,40,2048]{2,1,0:T(8,128)(2,1)} all-to-all(bf16[8,40,2048]{2,1,0:T(8,128)(2,1)S(1)} %bitcast.102), channel_id=1, replica_groups=mesh['ep'=8,'tp'=4] {'ep'}, dimensions={0} | all-to-all | bytes 2621440 | tf_op jit(solution)/shard_map/all_to_all | solution.py:115
  51.8 0.0 all-gather.8.cloned.1.call-update
  51.8 0.0 all-gather.4.cloned.1.call-start
  51.9 0.8 copy.56
  52.7 0.0 all-gather.4.cloned.1.call-update
  52.8 0.0 all-gather.6.cloned.1.call-start
  52.8 0.8 copy.58
  53.7 0.0 all-gather.6.cloned.1.call-update
  53.7 0.0 reduce-scatter.5.cloned.1.call-start
  53.7 37.7 %all-gather.8.cloned.1.call-done = bf16[1280,2048]{1,0:T(8,128)(2,1)} async-done(((bf16[320,2048]{1,0:T(8,128)(2,1)}), bf16[1280,2048]{1,0:T(8,128)(2,1)}) %all-gather.8.cloned.1.call-update) | async-done | bytes 5242896 | tf_op jit(solution)/shard_map/all_gather | solution.py:116
  91.4 10.0 %fusion.17 = f32[1280,896]{1,0:T(8,128)} fusion(bf16[1280,2048]{1,0:T(8,128)(2,1)} %all-gather.8.cloned.1.call-done, bf16[1,2048,896]{2,1,0:T(8,128)(2,1)} %param.25), kind=kOutput, calls=%fused_computation.25 | convolution fusion | flops 4697620480 | bytes 13500416 | tf_op jit(solution)/shard_map/dot_general | solution.py:119
  101.4 17.6 %convolution_convert_fusion = bf16[1280,2048]{1,0:T(8,128)(2,1)} fusion(bf16[1,896,2048]{2,1,0:T(8,128)(2,1)} %param.27, f32[1280,896]{1,0:T(8,128)} %fusion.17, bf16[1280,2048]{1,0:T(8,128)(2,1)} %all-gather.8.cloned.1.call-done, bf16[1,2048,896]{2,1,0:T(8,128)(2,1)} %param.26), kind=kOutput, calls=%fused_computation.20 | convolution fusion | flops 9404743680 | bytes 22413312 | tf_op jit(solution)/shard_map/dot_general | solution.py:132
  119.0 0.0 reduce-scatter.5.cloned.1.call-update
  119.0 0.0 reduce-scatter.3.cloned.1.call-start
  119.1 0.8 copy-done.3
  119.9 0.1 copy.57
  120.1 24.3 %all-gather.4.cloned.1.call-done = bf16[4096,256]{0,1:T(8,128)(2,1)} async-done(((bf16[512,256]{0,1:T(8,128)(2,1)}), bf16[4096,256]{0,1:T(8,128)(2,1)}) %all-gather.4.cloned.1.call-update) | async-done | bytes 2097168 | tf_op jit(solution)/shard_map/all_gather | solution.py:63
  144.4 51.2 %all-gather.6.cloned.1.call-done = bf16[4096,256]{0,1:T(8,128)(2,1)} async-done(((bf16[512,256]{0,1:T(8,128)(2,1)}), bf16[4096,256]{0,1:T(8,128)(2,1)}) %all-gather.6.cloned.1.call-update) | async-done | bytes 2097168 | tf_op jit(solution)/shard_map/all_gather | solution.py:64
  195.6 46.9 %while.18 = (s32[]{:T(128)}, f32[2,2,512]{2,1,0:T(2,128)S(1)}, f32[2,2,512]{2,1,0:T(2,128)S(1)}, f32[2,2,512,128]{2,3,0,1:T(8,128)S(1)}, bf16[4096,256]{0,1:T(8,...) while((s32[]{:T(128)}, f32[2,2,512]{2,1,0:T(2,128)S(1)}, ...), condition=%wide.region_3.0_spmd.clone, body=%wide.region_0.0_spmd.clone.sunk | while | flops 818685952 | bytes 30810288 | solution.py:78
  195.6 1.3 constant_dynamic-slice_fusion.3
  196.9 4.6 %bitcast_reduce_fusion.2 = (f32[2,2,512]{2,1,0:T(2,128)S(1)}, f32[2,2,1024,512]{3,2,1,0:T(8,128)}) fusion(bf16[512,2,2,64]{0,3,1,2:T(8,128)(2,1)S(1)} %get-tuple-element.284, bf16[1024,2,2,64]{0,3,2,1:T(8,128)(2,1)S(1)} %bitcast.99), kind=kOutput, calls=%fused_computation.2.clone.1 | convolution fusion | flops 272627712 | bytes 9183232 | tf_op jit(solution)/shard_map/while/body/eval_jaxpr/qhid,khid->ihqk/dot_general | solution.py:43
  201.5 5.4 %fusion.66 = (bf16[2,2,512,1024]{2,3,1,0:T(8,128)(2,1)S(1)}, f32[2,2,512]{2,1,0:T(2,128)S(1)}) fusion(f32[2,2,1024,512]{3,2,1,0:T(8,128)} %get-tuple-element.251, f32[2,2,512]{2,1,0:T(2,128)S(1)} %fusion.65), kind=kLoop, calls=%fused_computation.4.clone.1 | loop fusion | flops 8386560 | bytes 12599296 | tf_op jit(solution)/shard_map/while/body/eval_jaxpr/convert_element_type | solution.py:52
  207.0 0.9 fusion.68
  207.9 1.3 constant_dynamic-slice_fusion.3
  209.2 4.6 %bitcast_reduce_fusion.2 = (f32[2,2,512]{2,1,0:T(2,128)S(1)}, f32[2,2,1024,512]{3,2,1,0:T(8,128)}) fusion(bf16[512,2,2,64]{0,3,1,2:T(8,128)(2,1)S(1)} %get-tuple-element.284, bf16[1024,2,2,64]{0,3,2,1:T(8,128)(2,1)S(1)} %bitcast.99), kind=kOutput, calls=%fused_computation.2.clone.1 | convolution fusion | flops 272627712 | bytes 9183232 | tf_op jit(solution)/shard_map/while/body/eval_jaxpr/qhid,khid->ihqk/dot_general | solution.py:43
  213.9 5.1 %fusion.66 = (bf16[2,2,512,1024]{2,3,1,0:T(8,128)(2,1)S(1)}, f32[2,2,512]{2,1,0:T(2,128)S(1)}) fusion(f32[2,2,1024,512]{3,2,1,0:T(8,128)} %get-tuple-element.251, f32[2,2,512]{2,1,0:T(2,128)S(1)} %fusion.65), kind=kLoop, calls=%fused_computation.4.clone.1 | loop fusion | flops 8386560 | bytes 12599296 | tf_op jit(solution)/shard_map/while/body/eval_jaxpr/convert_element_type | solution.py:52
  219.1 0.9 fusion.68
  220.0 1.3 constant_dynamic-slice_fusion.3
  221.3 4.6 %bitcast_reduce_fusion.2 = (f32[2,2,512]{2,1,0:T(2,128)S(1)}, f32[2,2,1024,512]{3,2,1,0:T(8,128)}) fusion(bf16[512,2,2,64]{0,3,1,2:T(8,128)(2,1)S(1)} %get-tuple-element.284, bf16[1024,2,2,64]{0,3,2,1:T(8,128)(2,1)S(1)} %bitcast.99), kind=kOutput, calls=%fused_computation.2.clone.1 | convolution fusion | flops 272627712 | bytes 9183232 | tf_op jit(solution)/shard_map/while/body/eval_jaxpr/qhid,khid->ihqk/dot_general | solution.py:43
  225.9 4.3 %fusion.66 = (bf16[2,2,512,1024]{2,3,1,0:T(8,128)(2,1)S(1)}, f32[2,2,512]{2,1,0:T(2,128)S(1)}) fusion(f32[2,2,1024,512]{3,2,1,0:T(8,128)} %get-tuple-element.251, f32[2,2,512]{2,1,0:T(2,128)S(1)} %fusion.65), kind=kLoop, calls=%fused_computation.4.clone.1 | loop fusion | flops 8386560 | bytes 12599296 | tf_op jit(solution)/shard_map/while/body/eval_jaxpr/convert_element_type | solution.py:52
  230.3 0.9 fusion.68
  231.3 1.3 constant_dynamic-slice_fusion.3
  232.6 4.6 %bitcast_reduce_fusion.2 = (f32[2,2,512]{2,1,0:T(2,128)S(1)}, f32[2,2,1024,512]{3,2,1,0:T(8,128)}) fusion(bf16[512,2,2,64]{0,3,1,2:T(8,128)(2,1)S(1)} %get-tuple-element.284, bf16[1024,2,2,64]{0,3,2,1:T(8,128)(2,1)S(1)} %bitcast.99), kind=kOutput, calls=%fused_computation.2.clone.1 | convolution fusion | flops 272627712 | bytes 9183232 | tf_op jit(solution)/shard_map/while/body/eval_jaxpr/qhid,khid->ihqk/dot_general | solution.py:43
  237.2 4.3 %fusion.66 = (bf16[2,2,512,1024]{2,3,1,0:T(8,128)(2,1)S(1)}, f32[2,2,512]{2,1,0:T(2,128)S(1)}) fusion(f32[2,2,1024,512]{3,2,1,0:T(8,128)} %get-tuple-element.251, f32[2,2,512]{2,1,0:T(2,128)S(1)} %fusion.65), kind=kLoop, calls=%fused_computation.4.clone.1 | loop fusion | flops 8386560 | bytes 12599296 | tf_op jit(solution)/shard_map/while/body/eval_jaxpr/convert_element_type | solution.py:52
  241.5 0.9 fusion.68
  242.5 0.1 broadcast_divide_fusion
  242.6 0.2 multiply_reduce_fusion.1
  242.8 0.0 copy-start.4
  242.8 0.0 copy-start.5
  242.9 2.2 bitcast_convert_fusion
  245.1 0.0 reduce-scatter.3.cloned.1.call-update
  245.1 2.4 reduce-scatter.5.cloned.1.call-done
  247.5 5.5 %all-to-all-start.1 = ((bf16[8,40,2048]{2,1,0:T(8,128)(2,1)}), bf16[8,40,2048]{2,1,0:T(8,128)(2,1)S(1)}, u32[]{:S(2)}, u32[]{:S(2)}) async-start(bf16[8,40,2048]{2,1,0:T(8,128)(2,1)} %bitcast.103), calls=%async_computation.3 | async-start | bytes 2621440 | tf_op jit(solution)/shard_map/all_to_all | solution.py:137
  253.1 0.1 copy.68
  253.2 0.1 mul.155
  253.3 0.1 copy.67
  253.5 0.1 copy.63
  253.7 30.6 %all-to-all-done.1 = bf16[8,40,2048]{2,1,0:T(8,128)(2,1)S(1)} async-done(((bf16[8,40,2048]{2,1,0:T(8,128)(2,1)}), bf16[8,40,2048]{2,1,0:T(8,128)(2,1)S(1)}, u32[]{:S(2)}, u32[]{:S(2)}) %all-to-all-start.1) | async-done | bytes 1310752 | tf_op jit(solution)/shard_map/all_to_all | solution.py:137
  284.3 1.4 gather_fusion
  285.6 0.7 gather.7
  286.4 4.9 %multiply_reduce_fusion = bf16[128,2048]{1,0:T(8,128)(2,1)} fusion(bf16[128,2,2048]{2,1,0:T(2,128)(2,1)S(1)} %gather.7, pred[128,2]{1,0:T(8,128)(4,1)S(1)} %copy.67, f32[128,2]{1,0:T(8,128)S(1)} %copy.63), kind=kLoop, calls=%fused_computation.28 | loop fusion | flops 1835008 | bytes 1574144 | tf_op jit(solution)/shard_map/reduce_sum | solution.py:147
  (46 shorter events, 0.4 us)
Async XLA Ops:
  7.2 235.7 %copy-start = (bf16[256,2048]{1,0:T(8,128)(2,1)S(1)}, bf16[256,2048]{1,0:T(8,128)(2,1)}, u32[]{:S(2)}) copy-start(bf16[256,2048]{1,0:T(8,128)(2,1)} %param.20) | copy-start | bytes 3145732
  7.2 44.7 %copy-start.1 = (bf16[512,256]{1,0:T(8,128)(2,1)S(1)}, bf16[512,256]{1,0:T(8,128)(2,1)}, u32[]{:S(2)}) copy-start(bf16[512,256]{1,0:T(8,128)(2,1)} %param.16) | copy-start | bytes 786436
  7.2 45.6 %copy-start.2 = (bf16[512,256]{1,0:T(8,128)(2,1)S(1)}, bf16[512,256]{1,0:T(8,128)(2,1)}, u32[]{:S(2)}) copy-start(bf16[512,256]{1,0:T(8,128)(2,1)} %param.17) | copy-start | bytes 786436
  7.2 84.2 %all-gather.8.cloned.1.call-start = ((), (), s32[]{:S(2)}) async-start(), calls=%async_computation.7 | async-start | bytes 6553600 | tf_op jit(solution)/shard_map/all_gather | solution.py:116
  51.8 92.6 %all-gather.4.cloned.1.call-start = ((), (), s32[]{:S(2)}) async-start(), calls=%async_computation.4 | async-start | bytes 2359296 | tf_op jit(solution)/shard_map/all_gather | solution.py:63
  52.8 142.8 %all-gather.6.cloned.1.call-start = ((), (), s32[]{:S(2)}) async-start(), calls=%async_computation.5 | async-start | bytes 2359296 | tf_op jit(solution)/shard_map/all_gather | solution.py:64
  53.7 193.9 %reduce-scatter.5.cloned.1.call-start = ((), (), s32[]{:S(2)}) async-start(), calls=%async_computation.8 | async-start | bytes 6553600 | tf_op jit(solution)/shard_map/reduce_scatter | solution.py:131
  119.0 0.9 copy-start.3
  119.0 172.3 %reduce-scatter.3.cloned.1.call-start = ((), (), s32[]{:S(2)}) async-start(), calls=%async_computation.6 | async-start | bytes 2621440 | tf_op jit(solution)/shard_map/reduce_scatter | solution.py:123
  195.6 47.0 %copy-start.6 = (f32[2]{0:T(128)S(1)}, f32[2]{0:T(128)}, u32[]{:S(2)}) copy-start(f32[2]{0:T(128)} %param.18) | copy-start | bytes 28
  195.6 47.3 %copy-start.7 = (f32[128]{0:T(128)S(1)}, f32[128]{0:T(128)}, u32[]{:S(2)}) copy-start(f32[128]{0:T(128)} %param.19) | copy-start | bytes 1540
  242.8 10.2 %copy-start.4 = (s32[128,2]{0,1:T(2,128)S(1)}, s32[128,2]{0,1:T(2,128)}, u32[]{:S(2)}) copy-start(s32[128,2]{0,1:T(2,128)} %param.23) | copy-start | bytes 3076
  242.8 10.6 %copy-start.5 = (f32[128,2]{0,1:T(2,128)S(1)}, f32[128,2]{0,1:T(2,128)}, u32[]{:S(2)}) copy-start(f32[128,2]{0,1:T(2,128)} %param.24) | copy-start | bytes 3076
  247.5 36.7 %all-to-all-start.1 = ((bf16[8,40,2048]{2,1,0:T(8,128)(2,1)}), bf16[8,40,2048]{2,1,0:T(8,128)(2,1)S(1)}, u32[]{:S(2)}, u32[]{:S(2)}) async-start(bf16[8,40,2048]{2,1,0:T(8,128)(2,1)} %bitcast.103), calls=%async_computation.3 | async-start | bytes 2621440 | tf_op jit(solution)/shard_map/all_to_all | solution.py:137
Sparse Core Ops, SparseCore 0:
  51.9 39.4 all-gather.7
  94.0 50.3 all-gather.3
  147.0 48.5 all-gather.5
  198.0 49.5 reduce-scatter.4
  250.5 31.1 reduce-scatter.2
where the time goes:
time: 298 us
  waiting for transfers between devices  146 us (49%)
  matrix products  53.6 us (18%)
  blocking collectives  38.6 us (13%)
  other arithmetic  27.3 us (9%)
  between operations  14 us (5%)
  local copies, waits for them, and re-layouts  12.1 us (4%)
  starting transfers between devices  5.71 us (2%)
    all_gather x1, waiting for transfers between devices, per_device(): value_piece = lax.all_gather(value_rows, 'ep', axis=0, tiled=True)  51.2 us
    all_to_all x1, blocking collectives, per_device(): lax.all_to_all(outgoing, 'ep', split_axis=0, concat_axis=0, tiled=True)  38.6 us
    all_gather x1, waiting for transfers between devices, per_device(): lax.all_gather(arrived.reshape(experts_all * slot_count, model_width), 't...  37.7 us
    all_to_all x1, waiting for transfers between devices, per_device(): lax.all_to_all(expert_sum.reshape(experts_all, slot_count, model_width),...  30.6 us
    all_gather x1, waiting for transfers between devices, per_device(): key_piece = lax.all_gather(key_rows, 'ep', axis=0, tiled=True)  24.3 us
    convert_element_type x4, other arithmetic, attend_block(): weights.astype(jnp.bfloat16)  19.1 us
    dot_general x4, matrix products, attend_block(): jnp.einsum('qhid,khid->ihqk', query_maps, key_maps, preferred_element_typ...  18.5 us
    dot_general x1, matrix products, per_device(): jnp.dot(hidden, down_local, preferred_element_type=jnp.float32)  17.6 us
  transfers between devices with their start and end apart: 6, of which 5 were waited for; matrix products, arithmetic and copies ran while one was open for 29% of the time, Pallas kernels for 0%

commit v1 on v0

--- a/solution.py
+++ b/solution.py
@@ -61,7 +61,12 @@
         jnp.zeros((2, local_heads, local_rows, value_size), jnp.float32),
     )
     key_piece = lax.all_gather(key_rows, "ep", axis=0, tiled=True)
-    value_piece = lax.all_gather(value_rows, "ep", axis=0, tiled=True)
+    ring = [value_rows]
+    for hop in range(7):
+        ring.append(lax.ppermute(ring[-1], "ep", [(dev, (dev + 1) % 8) for dev in range(8)]))
+    value_piece = jnp.roll(
+        jnp.concatenate(ring[::-1], axis=0), (lax.axis_index("ep") + 1) * ring[0].shape[0], axis=0
+    )
     length = key_piece.shape[0]
     block_rows = length
     while block_rows > 1024 and block_rows % 2 == 0:

time: 298 us -> 267 us (0.90)
  waiting for transfers between devices: 146 us -> 93.2 us
  local copies, waits for them, and re-layouts: 12.1 us -> 35.9 us
    ppermute x0 -> x7, waiting for transfers between devices: none -> 63.4 us  [per_device(): lax.ppermute(ring[-1], 'ep', [(dev, (dev + 1) % 8) for dev in range(8)])]
    all_gather x1 -> x0, waiting for transfers between devices: 51.2 us -> none  [per_device(): value_piece = lax.all_gather(value_rows, 'ep', axis=0, tiled=True)]
    all_gather x1, waiting for transfers between devices: 37.7 us -> 0.01 us  [per_device(): lax.all_gather(arrived.reshape(experts_all * slot_count, model_width), 't...]
    all_gather x1, waiting for transfers between devices: 24.3 us -> 0.01 us  [per_device(): key_piece = lax.all_gather(key_rows, 'ep', axis=0, tiled=True)]
    unnamed x21 -> x38, local copies, waits for them, and re-layouts: 3.62 us -> 23.5 us
    dynamic_slice x0 -> x1, local copies, waits for them, and re-layouts: none -> 3.16 us  [per_device(): jnp.roll(jnp.concatenate(ring[::-1], axis=0), (lax.axis_index('ep') + 1)...]
  transfers between devices with their start and end apart: 6 -> 12, of which waited for: 5 -> 8; matrix products, arithmetic and copies ran while one was open for 29% -> 41% of each run, Pallas kernels for 0% -> 0%
where the time goes in v1:
time: 267 us
  waiting for transfers between devices  93.2 us (35%)
  matrix products  54 us (20%)
  blocking collectives  38.6 us (14%)
  local copies, waits for them, and re-layouts  35.9 us (13%)
  other arithmetic  25.3 us (9%)
  between operations  14.1 us (5%)
  starting transfers between devices  5.41 us (2%)
    ppermute x7, waiting for transfers between devices, per_device(): lax.ppermute(ring[-1], 'ep', [(dev, (dev + 1) % 8) for dev in range(8)])  63.4 us
    all_to_all x1, blocking collectives, per_device(): lax.all_to_all(outgoing, 'ep', split_axis=0, concat_axis=0, tiled=True)  38.6 us
    all_to_all x1, waiting for transfers between devices, per_device(): lax.all_to_all(expert_sum.reshape(experts_all, slot_count, model_width),...  29.7 us
    unnamed x38, local copies, waits for them, and re-layouts  23.5 us
    dot_general x4, matrix products, attend_block(): jnp.einsum('qhid,khid->ihqk', query_maps, key_maps, preferred_element_typ...  18.6 us
    dot_general x1, matrix products, per_device(): jnp.dot(hidden, down_local, preferred_element_type=jnp.float32)  17.8 us
    convert_element_type x4, other arithmetic, attend_block(): weights.astype(jnp.bfloat16)  17.2 us
    dot_general x1, matrix products, per_device(): gate_part = jnp.dot(segment, gate_local, preferred_element_type=jnp.float32)  10 us
  transfers between devices with their start and end apart: 12, of which 8 were waited for; matrix products, arithmetic and copies ran while one was open for 41% of the time, Pallas kernels for 0%

profile of v1, /device:TPU:0, one launch (start us, length us, event | category | flops | bytes accessed | tf_op | source)
XLA Modules:
  0.0 266.7 jit_solution(305701796914433798)
XLA Ops:
  7.2 0.9 copy.72
  8.4 0.6 reduce-window.6
  9.0 0.2 slice_reduce_fusion
  9.4 0.1 reduce_sum.65
  9.6 0.7 compare_and_fusion
  10.3 1.2 fusion.19
  11.6 1.6 convolution_convert_fusion.1
  13.2 38.6 %all_to_all.10 = bf16[8,40,2048]{2,1,0:T(8,128)(2,1)} all-to-all(bf16[8,40,2048]{2,1,0:T(8,128)(2,1)S(1)} %bitcast.102), channel_id=1, replica_groups=mesh['ep'=8,'tp'=4] {'ep'}, dimensions={0} | all-to-all | bytes 2621440 | tf_op jit(solution)/shard_map/all_to_all | solution.py:120
  51.9 0.1 copy.64
  52.0 1.5 collective-permute-start
  53.5 8.1 %collective-permute-done = bf16[512,256]{0,1:T(8,128)(2,1)S(1)} collective-permute-done((bf16[512,256]{0,1:T(8,128)(2,1)S(1)}, bf16[512,256]{0,1:T(8,128)(2,1)S(1)}, u32[]{:S(2)}, u32[]{:S(2)}) %collective-permute-start) | collective-permute-done | bytes 262176 | tf_op jit(solution)/shard_map/ppermute | solution.py:66
  61.6 9.1 %collective-permute-done.1 = bf16[512,256]{0,1:T(8,128)(2,1)S(1)} collective-permute-done((bf16[512,256]{0,1:T(8,128)(2,1)S(1)}, bf16[512,256]{0,1:T(8,128)(2,1)S(1)}, u32[]{:S(2)}, u32[]{:S(2)}) %collective-permute-start.1) | collective-permute-done | bytes 262176 | tf_op jit(solution)/shard_map/ppermute | solution.py:66
  70.7 9.1 %collective-permute-done.2 = bf16[512,256]{0,1:T(8,128)(2,1)S(1)} collective-permute-done((bf16[512,256]{0,1:T(8,128)(2,1)S(1)}, bf16[512,256]{0,1:T(8,128)(2,1)S(1)}, u32[]{:S(2)}, u32[]{:S(2)}) %collective-permute-start.2) | collective-permute-done | bytes 262176 | tf_op jit(solution)/shard_map/ppermute | solution.py:66
  79.8 9.4 %collective-permute-done.3 = bf16[512,256]{0,1:T(8,128)(2,1)S(1)} collective-permute-done((bf16[512,256]{0,1:T(8,128)(2,1)S(1)}, bf16[512,256]{0,1:T(8,128)(2,1)S(1)}, u32[]{:S(2)}, u32[]{:S(2)}) %collective-permute-start.3) | collective-permute-done | bytes 262176 | tf_op jit(solution)/shard_map/ppermute | solution.py:66
  89.2 10.6 %collective-permute-done.4 = bf16[512,256]{0,1:T(8,128)(2,1)S(1)} collective-permute-done((bf16[512,256]{0,1:T(8,128)(2,1)S(1)}, bf16[512,256]{0,1:T(8,128)(2,1)S(1)}, u32[]{:S(2)}, u32[]{:S(2)}) %collective-permute-start.4) | collective-permute-done | bytes 262176 | tf_op jit(solution)/shard_map/ppermute | solution.py:66
  99.8 11.5 %collective-permute-done.5 = bf16[512,256]{0,1:T(8,128)(2,1)} collective-permute-done((bf16[512,256]{0,1:T(8,128)(2,1)S(1)}, bf16[512,256]{0,1:T(8,128)(2,1)}, u32[]{:S(2)}, u32[]{:S(2)}) %collective-permute-start.5) | collective-permute-done | bytes 262176 | tf_op jit(solution)/shard_map/ppermute | solution.py:66
  111.3 0.8 copy.62
  112.3 1.8 copy.63
  114.1 1.0 copy.67
  115.1 5.6 %collective-permute-done.6 = bf16[512,256]{0,1:T(8,128)(2,1)} collective-permute-done((bf16[512,256]{0,1:T(8,128)(2,1)}, bf16[512,256]{0,1:T(8,128)(2,1)}, u32[]{:S(2)}, u32[]{:S(2)}) %collective-permute-start.6) | collective-permute-done | bytes 262176 | tf_op jit(solution)/shard_map/ppermute | solution.py:66
  120.7 1.7 constant_dynamic-update-slice_fusion.15
  122.4 1.7 constant_dynamic-update-slice_fusion.14
  124.1 1.7 constant_dynamic-update-slice_fusion.13
  125.9 1.7 constant_dynamic-update-slice_fusion.12
  127.6 0.8 constant_dynamic-update-slice_fusion.11
  128.3 0.8 constant_dynamic-update-slice_fusion.10
  129.1 0.7 constant_dynamic-update-slice_fusion.9
  129.8 0.7 constant_dynamic-update-slice_fusion.8
  130.6 10.0 %fusion.17 = f32[1280,896]{1,0:T(8,128)} fusion(bf16[1280,2048]{1,0:T(8,128)(2,1)} %all-gather.5.cloned.1.call-done, bf16[1,2048,896]{2,1,0:T(8,128)(2,1)} %param.25), kind=kOutput, calls=%fused_computation.25 | convolution fusion | flops 4697620480 | bytes 13500416 | tf_op jit(solution)/shard_map/dot_general | solution.py:124
  140.6 17.8 %convolution_convert_fusion = bf16[1280,2048]{1,0:T(8,128)(2,1)} fusion(bf16[1,896,2048]{2,1,0:T(8,128)(2,1)} %param.27, f32[1280,896]{1,0:T(8,128)} %fusion.17, bf16[1280,2048]{1,0:T(8,128)(2,1)} %all-gather.5.cloned.1.call-done, bf16[1,2048,896]{2,1,0:T(8,128)(2,1)} %param.26), kind=kOutput, calls=%fused_computation.20 | convolution fusion | flops 9404743680 | bytes 22413312 | tf_op jit(solution)/shard_map/dot_general | solution.py:137
  158.4 0.2 reduce-scatter.3.cloned.1.call-start
  158.6 1.7 constant_dynamic-update-slice_fusion.7
  160.3 1.7 constant_dynamic-update-slice_fusion.6
  162.0 1.7 constant_dynamic-update-slice_fusion.5
  163.7 1.7 constant_dynamic-update-slice_fusion.4
  165.3 0.7 constant_dynamic-update-slice_fusion.3
  166.1 0.7 constant_dynamic-update-slice_fusion.2
  166.8 0.8 constant_dynamic-update-slice_fusion.1
  167.6 0.8 constant_dynamic-update-slice_fusion
  168.4 3.2 %constant_dynamic-slice_fusion.2 = bf16[4096,256]{0,1:T(8,128)(2,1)} fusion(bf16[8192,256]{0,1:T(8,128)(2,1)} %constant_dynamic-update-slice_fusion, s32[]{:T(128)S(6)} %select_n.44), kind=kLoop, calls=%fused_computation.82 | loop fusion | bytes 4194308 | tf_op jit(solution)/shard_map/jit(_roll_dynamic)/dynamic_slice | solution.py:67
  171.5 45.0 %while.18 = (s32[]{:T(128)}, f32[2,2,512]{2,1,0:T(2,128)S(1)}, f32[2,2,512]{2,1,0:T(2,128)S(1)}, f32[2,2,512,128]{2,3,0,1:T(8,128)S(1)}, bf16[4096,256]{0,1:T(8,...) while((s32[]{:T(128)}, f32[2,2,512]{2,1,0:T(2,128)S(1)}, ...), condition=%wide.region_3.4_spmd.clone, body=%wide.region_0.3_spmd.clone.sunk | while | flops 818685952 | bytes 30810280 | solution.py:83
  171.5 1.3 constant_dynamic-slice_fusion.4
  172.8 4.8 %bitcast_reduce_fusion.2 = (f32[2,2,512]{2,1,0:T(2,128)S(1)}, f32[2,2,1024,512]{3,2,1,0:T(8,128)}) fusion(bf16[512,2,2,64]{0,3,1,2:T(8,128)(2,1)S(1)} %get-tuple-element.284, bf16[1024,2,2,64]{0,3,2,1:T(8,128)(2,1)S(1)} %bitcast.99), kind=kOutput, calls=%fused_computation.2.clone.1 | convolution fusion | flops 272627712 | bytes 9183232 | tf_op jit(solution)/shard_map/while/body/eval_jaxpr/qhid,khid->ihqk/dot_general | solution.py:43
  177.6 4.3 %fusion.66 = (bf16[2,2,512,1024]{2,3,1,0:T(8,128)(2,1)S(1)}, f32[2,2,512]{2,1,0:T(2,128)S(1)}) fusion(f32[2,2,1024,512]{3,2,1,0:T(8,128)} %get-tuple-element.251, f32[2,2,512]{2,1,0:T(2,128)S(1)} %fusion.65), kind=kLoop, calls=%fused_computation.4.clone.1 | loop fusion | flops 8386560 | bytes 12599296 | tf_op jit(solution)/shard_map/while/body/eval_jaxpr/convert_element_type | solution.py:52
  182.0 0.9 fusion.68
  182.9 1.3 constant_dynamic-slice_fusion.4
  184.2 4.6 %bitcast_reduce_fusion.2 = (f32[2,2,512]{2,1,0:T(2,128)S(1)}, f32[2,2,1024,512]{3,2,1,0:T(8,128)}) fusion(bf16[512,2,2,64]{0,3,1,2:T(8,128)(2,1)S(1)} %get-tuple-element.284, bf16[1024,2,2,64]{0,3,2,1:T(8,128)(2,1)S(1)} %bitcast.99), kind=kOutput, calls=%fused_computation.2.clone.1 | convolution fusion | flops 272627712 | bytes 9183232 | tf_op jit(solution)/shard_map/while/body/eval_jaxpr/qhid,khid->ihqk/dot_general | solution.py:43
  188.8 4.3 %fusion.66 = (bf16[2,2,512,1024]{2,3,1,0:T(8,128)(2,1)S(1)}, f32[2,2,512]{2,1,0:T(2,128)S(1)}) fusion(f32[2,2,1024,512]{3,2,1,0:T(8,128)} %get-tuple-element.251, f32[2,2,512]{2,1,0:T(2,128)S(1)} %fusion.65), kind=kLoop, calls=%fused_computation.4.clone.1 | loop fusion | flops 8386560 | bytes 12599296 | tf_op jit(solution)/shard_map/while/body/eval_jaxpr/convert_element_type | solution.py:52
  193.1 0.9 fusion.68
  194.1 1.3 constant_dynamic-slice_fusion.4
  195.4 4.6 %bitcast_reduce_fusion.2 = (f32[2,2,512]{2,1,0:T(2,128)S(1)}, f32[2,2,1024,512]{3,2,1,0:T(8,128)}) fusion(bf16[512,2,2,64]{0,3,1,2:T(8,128)(2,1)S(1)} %get-tuple-element.284, bf16[1024,2,2,64]{0,3,2,1:T(8,128)(2,1)S(1)} %bitcast.99), kind=kOutput, calls=%fused_computation.2.clone.1 | convolution fusion | flops 272627712 | bytes 9183232 | tf_op jit(solution)/shard_map/while/body/eval_jaxpr/qhid,khid->ihqk/dot_general | solution.py:43
  200.0 4.4 %fusion.66 = (bf16[2,2,512,1024]{2,3,1,0:T(8,128)(2,1)S(1)}, f32[2,2,512]{2,1,0:T(2,128)S(1)}) fusion(f32[2,2,1024,512]{3,2,1,0:T(8,128)} %get-tuple-element.251, f32[2,2,512]{2,1,0:T(2,128)S(1)} %fusion.65), kind=kLoop, calls=%fused_computation.4.clone.1 | loop fusion | flops 8386560 | bytes 12599296 | tf_op jit(solution)/shard_map/while/body/eval_jaxpr/convert_element_type | solution.py:52
  204.4 0.9 fusion.68
  205.4 1.3 constant_dynamic-slice_fusion.4
  206.6 4.6 %bitcast_reduce_fusion.2 = (f32[2,2,512]{2,1,0:T(2,128)S(1)}, f32[2,2,1024,512]{3,2,1,0:T(8,128)}) fusion(bf16[512,2,2,64]{0,3,1,2:T(8,128)(2,1)S(1)} %get-tuple-element.284, bf16[1024,2,2,64]{0,3,2,1:T(8,128)(2,1)S(1)} %bitcast.99), kind=kOutput, calls=%fused_computation.2.clone.1 | convolution fusion | flops 272627712 | bytes 9183232 | tf_op jit(solution)/shard_map/while/body/eval_jaxpr/qhid,khid->ihqk/dot_general | solution.py:43
  211.2 4.3 %fusion.66 = (bf16[2,2,512,1024]{2,3,1,0:T(8,128)(2,1)S(1)}, f32[2,2,512]{2,1,0:T(2,128)S(1)}) fusion(f32[2,2,1024,512]{3,2,1,0:T(8,128)} %get-tuple-element.251, f32[2,2,512]{2,1,0:T(2,128)S(1)} %fusion.65), kind=kLoop, calls=%fused_computation.4.clone.1 | loop fusion | flops 8386560 | bytes 12599296 | tf_op jit(solution)/shard_map/while/body/eval_jaxpr/convert_element_type | solution.py:52
  215.6 0.9 fusion.68
  216.7 0.2 multiply_reduce_fusion.1
  216.9 2.2 bitcast_convert_fusion
  219.2 3.6 %all-to-all-start.1 = ((bf16[8,40,2048]{2,1,0:T(8,128)(2,1)}), bf16[8,40,2048]{2,1,0:T(8,128)(2,1)S(1)}, u32[]{:S(2)}, u32[]{:S(2)}) async-start(bf16[8,40,2048]{2,1,0:T(8,128)(2,1)} %bitcast.103), calls=%async_computation.3 | async-start | bytes 2621440 | tf_op jit(solution)/shard_map/all_to_all | solution.py:142
  223.4 29.7 %all-to-all-done.1 = bf16[8,40,2048]{2,1,0:T(8,128)(2,1)S(1)} async-done(((bf16[8,40,2048]{2,1,0:T(8,128)(2,1)}), bf16[8,40,2048]{2,1,0:T(8,128)(2,1)S(1)}, u32[]{:S(2)}, u32[]{:S(2)}) %all-to-all-start.1) | async-done | bytes 1310752 | tf_op jit(solution)/shard_map/all_to_all | solution.py:142
  253.1 1.4 gather_fusion
  254.5 0.7 gather.7
  255.2 4.9 %multiply_reduce_fusion = bf16[128,2048]{1,0:T(8,128)(2,1)} fusion(bf16[128,2,2048]{2,1,0:T(2,128)(2,1)S(1)} %gather.7, pred[128,2]{1,0:T(8,128)(4,1)S(1)} %copy.75, f32[128,2]{1,0:T(8,128)S(1)} %copy.71), kind=kLoop, calls=%fused_computation.28 | loop fusion | flops 1835008 | bytes 1574144 | tf_op jit(solution)/shard_map/reduce_sum | solution.py:152
  (76 shorter events, 1.7 us)
Async XLA Ops:
  7.2 209.7 %copy-start = (bf16[256,2048]{1,0:T(8,128)(2,1)S(1)}, bf16[256,2048]{1,0:T(8,128)(2,1)}, u32[]{:S(2)}) copy-start(bf16[256,2048]{1,0:T(8,128)(2,1)} %param.20) | copy-start | bytes 3145732
  7.2 44.7 %copy-start.3 = (bf16[512,256]{1,0:T(8,128)(2,1)S(1)}, bf16[512,256]{1,0:T(8,128)(2,1)}, u32[]{:S(2)}) copy-start(bf16[512,256]{1,0:T(8,128)(2,1)} %param.17) | copy-start | bytes 786436
  7.2 104.1 %copy-start.4 = (bf16[512,256]{1,0:T(8,128)(2,1)S(1)}, bf16[512,256]{1,0:T(8,128)(2,1)}, u32[]{:S(2)}) copy-start(bf16[512,256]{1,0:T(8,128)(2,1)} %param.16) | copy-start | bytes 786436
  7.2 123.4 %all-gather.5.cloned.1.call-start = ((), (), s32[]{:S(2)}) async-start(), calls=%async_computation.6 | async-start | bytes 6553600 | tf_op jit(solution)/shard_map/all_gather | solution.py:121
  51.8 119.7 %all-gather.3.cloned.1.call-start = ((), (), s32[]{:S(2)}) async-start(), calls=%async_computation.4 | async-start | bytes 2359296 | tf_op jit(solution)/shard_map/all_gather | solution.py:63
  52.0 9.6 %collective-permute-start = (bf16[512,256]{0,1:T(8,128)(2,1)S(1)}, bf16[512,256]{0,1:T(8,128)(2,1)S(1)}, u32[]{:S(2)}, u32[]{:S(2)}) collective-permute-start(bf16[512,256]{0,1:T(8,128)(2,1)S(1)} %copy.64), channel_id=1, source_target_pairs={{0,4},{4,8},{8,12},{12,16},{16,20},{20,24},{24,28},{28,0},{1,5},{5... | collective-permute-start | bytes 786440 | tf_op jit(solution)/shard_map/ppermute | solution.py:66
  61.6 9.1 %collective-permute-start.1 = (bf16[512,256]{0,1:T(8,128)(2,1)S(1)}, bf16[512,256]{0,1:T(8,128)(2,1)S(1)}, u32[]{:S(2)}, u32[]{:S(2)}) collective-permute-start(bf16[512,256]{0,1:T(8,128)(2,1)S(1)} %collective-permute-done), channel_id=1, source_target_pairs={{0,4},{4,8},{8,12},{12,16},{16,20},{20,24},{24,28},{28,0},{1,5},{5... | collective-permute-start | bytes 786440 | tf_op jit(solution)/shard_map/ppermute | solution.py:66
  70.7 9.1 %collective-permute-start.2 = (bf16[512,256]{0,1:T(8,128)(2,1)S(1)}, bf16[512,256]{0,1:T(8,128)(2,1)S(1)}, u32[]{:S(2)}, u32[]{:S(2)}) collective-permute-start(bf16[512,256]{0,1:T(8,128)(2,1)S(1)} %collective-permute-done.1), channel_id=1, source_target_pairs={{0,4},{4,8},{8,12},{12,16},{16,20},{20,24},{24,28},{28,0},{1,5},{5... | collective-permute-start | bytes 786440 | tf_op jit(solution)/shard_map/ppermute | solution.py:66
  79.8 9.4 %collective-permute-start.3 = (bf16[512,256]{0,1:T(8,128)(2,1)S(1)}, bf16[512,256]{0,1:T(8,128)(2,1)S(1)}, u32[]{:S(2)}, u32[]{:S(2)}) collective-permute-start(bf16[512,256]{0,1:T(8,128)(2,1)S(1)} %collective-permute-done.2), channel_id=1, source_target_pairs={{0,4},{4,8},{8,12},{12,16},{16,20},{20,24},{24,28},{28,0},{1,5},{5... | collective-permute-start | bytes 786440 | tf_op jit(solution)/shard_map/ppermute | solution.py:66
  89.2 24.9 %copy-start.1 = (bf16[512,256]{0,1:T(8,128)(2,1)}, bf16[512,256]{0,1:T(8,128)(2,1)S(1)}, u32[]{:S(2)}) copy-start(bf16[512,256]{0,1:T(8,128)(2,1)S(1)} %collective-permute-done.3) | copy-start | bytes 786436
  89.2 10.6 %collective-permute-start.4 = (bf16[512,256]{0,1:T(8,128)(2,1)S(1)}, bf16[512,256]{0,1:T(8,128)(2,1)S(1)}, u32[]{:S(2)}, u32[]{:S(2)}) collective-permute-start(bf16[512,256]{0,1:T(8,128)(2,1)S(1)} %collective-permute-done.3), channel_id=1, source_target_pairs={{0,4},{4,8},{8,12},{12,16},{16,20},{20,24},{24,28},{28,0},{1,5},{5... | collective-permute-start | bytes 786440 | tf_op jit(solution)/shard_map/ppermute | solution.py:66
  99.8 12.4 %copy-start.2 = (bf16[512,256]{0,1:T(8,128)(2,1)}, bf16[512,256]{0,1:T(8,128)(2,1)S(1)}, u32[]{:S(2)}) copy-start(bf16[512,256]{0,1:T(8,128)(2,1)S(1)} %collective-permute-done.4) | copy-start | bytes 786436
  99.8 11.5 %collective-permute-start.5 = (bf16[512,256]{0,1:T(8,128)(2,1)S(1)}, bf16[512,256]{0,1:T(8,128)(2,1)}, u32[]{:S(2)}, u32[]{:S(2)}) collective-permute-start(bf16[512,256]{0,1:T(8,128)(2,1)S(1)} %collective-permute-done.4), channel_id=1, source_target_pairs={{0,4},{4,8},{8,12},{12,16},{16,20},{20,24},{24,28},{28,0},{1,5},{5... | collective-permute-start | bytes 786440 | tf_op jit(solution)/shard_map/ppermute | solution.py:66
  111.3 9.4 %collective-permute-start.6 = (bf16[512,256]{0,1:T(8,128)(2,1)}, bf16[512,256]{0,1:T(8,128)(2,1)}, u32[]{:S(2)}, u32[]{:S(2)}) collective-permute-start(bf16[512,256]{0,1:T(8,128)(2,1)} %collective-permute-done.5), channel_id=1, source_target_pairs={{0,4},{4,8},{8,12},{12,16},{16,20},{20,24},{24,28},{28,0},{1,5},{5... | collective-permute-start | bytes 786440 | tf_op jit(solution)/shard_map/ppermute | solution.py:66
  112.2 107.0 %reduce-scatter.5.cloned.1.call-start = ((), (), s32[]{:S(2)}) async-start(), calls=%async_computation.7 | async-start | bytes 6553600 | tf_op jit(solution)/shard_map/reduce_scatter | solution.py:136
  158.4 101.7 %reduce-scatter.3.cloned.1.call-start = ((), (), s32[]{:S(2)}) async-start(), calls=%async_computation.5 | async-start | bytes 2621440 | tf_op jit(solution)/shard_map/reduce_scatter | solution.py:128
  171.5 45.2 %copy-start.7 = (f32[2]{0:T(128)S(1)}, f32[2]{0:T(128)}, u32[]{:S(2)}) copy-start(f32[2]{0:T(128)} %param.18) | copy-start | bytes 28
  171.5 45.4 %copy-start.8 = (f32[128]{0:T(128)S(1)}, f32[128]{0:T(128)}, u32[]{:S(2)}) copy-start(f32[128]{0:T(128)} %param.19) | copy-start | bytes 1540
  216.9 5.9 %copy-start.5 = (s32[128,2]{0,1:T(2,128)S(1)}, s32[128,2]{0,1:T(2,128)}, u32[]{:S(2)}) copy-start(s32[128,2]{0,1:T(2,128)} %param.23) | copy-start | bytes 3076
  216.9 6.3 %copy-start.6 = (f32[128,2]{0,1:T(2,128)S(1)}, f32[128,2]{0,1:T(2,128)}, u32[]{:S(2)}) copy-start(f32[128,2]{0,1:T(2,128)} %param.24) | copy-start | bytes 3076
  219.2 33.9 %all-to-all-start.1 = ((bf16[8,40,2048]{2,1,0:T(8,128)(2,1)}), bf16[8,40,2048]{2,1,0:T(8,128)(2,1)S(1)}, u32[]{:S(2)}, u32[]{:S(2)}) async-start(bf16[8,40,2048]{2,1,0:T(8,128)(2,1)} %bitcast.103), calls=%async_computation.3 | async-start | bytes 2621440 | tf_op jit(solution)/shard_map/all_to_all | solution.py:142
Sparse Core Ops, SparseCore 0:
  51.9 39.4 all-gather.4
  112.3 51.7 all-gather.2
  166.6 49.5 reduce-scatter.4
  219.3 31.0 reduce-scatter.2
